TPU v7x, 32 devices: a whole 2x2x4 slice. The times are simulated.
32 devices in a mesh: fs: 4 (over y, x), tp: 8 (over z, core).
Axes of the slice: x: 2, y: 2, z: 4, core: 2. Of those that a mesh axis runs over, the one named last changes fastest.
Arguments:
- tokens: bfloat16 [4096, 2048], P(('fs', 'tp')), may hold values from -6 to 6
- norm_gain: float32 [2048], P('fs'), may hold values from 0.1 to 1.9
- gate_master: float32 [2048, 8192], P('fs', 'tp'), may hold values from -0.125 to 0.125
- up_master: float32 [2048, 8192], P('fs', 'tp'), may hold values from -0.125 to 0.125
- down_master: float32 [2048, 8192], P('fs', 'tp'), may hold values from -0.09375 to 0.09375
Outputs:
- mixed: bfloat16 [4096, 2048], P(('fs', 'tp'))
- gate_ready: bfloat16 [2048, 8192], P(None, 'tp')
- up_ready: bfloat16 [2048, 8192], P(None, 'tp')
- down_ready: bfloat16 [2048, 8192], P(None, 'tp')
All inputs are finite; a program needn't handle non-finite values.
Results may differ from a plain program's by a relative error of at most 0.0095.
Values may be sent and summed in bfloat16 or wider, within the bound.
A program may use at most 64 MiB of HBM per device.

v0:
```python
import functools

import jax
import jax.numpy as jnp
from jax import lax
from jax.experimental import pallas as pl
from jax.experimental.pallas import tpu as pltpu
from jax.sharding import PartitionSpec as P

MESH = pl.DeviceIdType.MESH
GATE, UP, DOWN = 0, 1, 2


def flip(index, bit):
    return index + bit - 2 * bit * ((index // bit) % 2)


def flip_all(index, mask, dims):
    for dim in range(dims):
        if mask >> dim & 1:
            index = flip(index, 1 << dim)
    return index


def span(bits):
    masks = [0]
    for bit in bits:
        masks += [mask | bit for mask in masks]
    return masks


def kernel(
    n_fs, n_z, dims, halves, pieces,
    tok_hbm, gain_hbm, gate_hbm, up_hbm, down_hbm,
    mixed, gate, up, down,
    tok_in, gain_row, gain, masters, tok, scale, gate_acc, up_acc, hidden, pair_own, pair_send, pair_recv, z_send, z_recv, ahead,
    w_sent, w_got, t_sent, t_got, s_sent, s_got, p_sent, p_got, z_sent, z_got, a_sent, a_got, loaded,
):
    fs, tp = lax.axis_index("fs"), lax.axis_index("tp")
    z, core = tp // 2, tp % 2
    sibling = z * 2 + 1 - core
    rows, cols = gate_hbm.shape
    part = rows // dims
    own_tok = tok_in.shape[0]
    half = n_z * own_tok
    total = 2 * half
    width = rows // pieces
    ready = (gate, up, down)

    loads = {}
    reads = [("gain", gain_hbm, gain_row)]
    for p in range(dims):
        mine = pl.ds(p * part, part)
        reads.append(((GATE, p), gate_hbm.at[mine, :], masters.at[GATE, mine, :]))
    for p in range(dims):
        mine = pl.ds(p * part, part)
        reads.append(((UP, p), up_hbm.at[mine, :], masters.at[UP, mine, :]))
    reads.append(("tok", tok_hbm, tok_in))
    reads.append(((DOWN, 0), down_hbm, masters.at[DOWN]))
    for n, (name, src, dst) in enumerate(reads):
        loads[name] = pltpu.make_async_copy(src, dst, loaded.at[n])
        loads[name].start()

    def z_peer(k):
        return ((z + k) % n_z) * 2 + core

    barrier = pltpu.get_barrier_semaphore()
    for dim in range(dims):
        pl.semaphore_signal(barrier, 1, device_id={"fs": flip(fs, 1 << dim)}, device_id_type=MESH)
    for k in range(1, n_z):
        pl.semaphore_signal(barrier, 1, device_id={"tp": z_peer(k)}, device_id_type=MESH)
    pl.semaphore_signal(barrier, 1, device_id={"tp": sibling}, device_id_type=MESH)
    pl.semaphore_wait(barrier, dims + n_z)

    loads["gain"].wait()
    for n in range(rows // 128):
        line = gain_row[:, n * 128:(n + 1) * 128]
        gain[n * 128:(n + 1) * 128, :] = jnp.transpose(jnp.broadcast_to(line, (128, 128)))

    cuts = (1, 1, halves)

    def block(w, mask, p, h):
        tall = part // cuts[w]
        start = flip_all(fs, mask, dims) * rows + p * part + h * tall
        return ready[w].at[pl.ds(pl.multiple_of(start, tall), tall), :]

    def order(p):
        return [1 << ((p + s) % dims) for s in range(dims)]

    arrivals = {
        (p, held | order(p)[stage]): stage
        for p in range(dims) for stage in range(dims) for held in span(order(p)[:stage])
    }
    started, arrived = [], set()

    def weight_copy(w, p, h, held, mask, stage):
        return pltpu.make_async_remote_copy(
            src_ref=block(w, held, p, h), dst_ref=block(w, held, p, h),
            send_sem=w_sent.at[w, p, h, mask], recv_sem=w_got.at[w, p, h, mask],
            device_id={"fs": flip(fs, order(p)[stage])}, device_id_type=MESH,
        )

    def launch(copy):
        copy.start()
        started.append(copy)

    def send(w, p, h, stage, held):
        launch(weight_copy(w, p, h, held, held | order(p)[stage], stage))

    def need(w, p, h, mask):
        if mask and (w, p, h, mask) not in arrived:
            arrived.add((w, p, h, mask))
            stage = arrivals[p, mask]
            weight_copy(w, p, h, mask, mask, stage).wait_recv()
            for later in range(stage + 1, dims):
                send(w, p, h, later, mask)

    def relays(ws):
        for stage in range(dims - 1):
            for w in ws:
                for p in range(dims):
                    for held in span(order(p)[:stage]):
                        for h in range(cuts[w]):
                            need(w, p, h, held | order(p)[stage])

    def prepare(w, p):
        mine = slice(p * part, (p + 1) * part)
        if (w, p) in loads:
            loads[w, p].wait()
        value = masters[w, mine, :]
        if w != DOWN:
            value = gain[mine, 0:1] * value
        ready[w][pl.ds(pl.multiple_of(fs * rows + p * part, part), part), :] = value.astype(jnp.bfloat16)

    for p in range(dims):
        prepare(GATE, p)
        send(GATE, p, 0, 0, 0)
    for p in range(dims):
        prepare(UP, p)
        send(UP, p, 0, 0, 0)

    def tok_rows(c, chip):
        start = (c * n_z + chip) * own_tok
        return tok.at[pl.ds(pl.multiple_of(start, own_tok), own_tok), :]

    def tok_z(k):
        return pltpu.make_async_remote_copy(
            src_ref=tok_in, dst_ref=tok_rows(core, z), send_sem=t_sent.at[k], recv_sem=t_got.at[k],
            device_id={"tp": z_peer(k)}, device_id_type=MESH,
        )

    def tok_sibling(k, src, slot):
        return pltpu.make_async_remote_copy(
            src_ref=src, dst_ref=slot, send_sem=s_sent.at[k], recv_sem=s_got.at[k],
            device_id={"tp": sibling}, device_id_type=MESH,
        )

    loads["tok"].wait()
    for k in range(1, n_z):
        launch(tok_z(k))
    launch(tok_sibling(0, tok_in, tok_rows(core, z)))
    for w in (GATE, UP):
        for p in range(dims):
            for stage in range(1, dims):
                send(w, p, 0, stage, 0)
    tok_rows(core, z)[...] = tok_in[...]
    for p in range(dims):
        prepare(DOWN, p)

    relays((GATE, UP))
    for stage in range(dims):
        for h in range(halves):
            for p in range(dims):
                send(DOWN, p, h, stage, 0)

    for k in range(1, n_z):
        slot = tok_rows(core, (z + n_z - k) % n_z)
        pltpu.make_async_remote_copy(
            src_ref=slot, dst_ref=slot, send_sem=t_sent.at[k], recv_sem=t_got.at[k],
            device_id={"tp": z_peer(k)}, device_id_type=MESH,
        ).wait_recv()
        launch(tok_sibling(k, slot, slot))
    for k in range(n_z):
        slot = tok_rows(1 - core, (z + n_z - k) % n_z)
        tok_sibling(k, slot, slot).wait_recv()

    tile_m, tile_n = min(256, total), min(512, cols)
    tile_s = min(64, total)

    @pl.loop(0, total // tile_s)
    def _(i):
        at = pl.ds(pl.multiple_of(i * tile_s, tile_s), tile_s)
        wide = tok[at, :].astype(jnp.float32)
        scale[at, :] = lax.rsqrt(jnp.mean(wide * wide, axis=1, keepdims=True) + 1e-06)

    for mask in range(n_fs):
        for w in (GATE, UP):
            for p in range(dims):
                need(w, p, 0, mask)
        owner = flip_all(fs, mask, dims)
        deep = pl.ds(pl.multiple_of(owner * rows, rows), rows)
        first, last = mask == 0, mask == n_fs - 1

        @pl.loop(0, (total // tile_m) * (cols // tile_n))
        def _(i):
            across = cols // tile_n
            at = pl.ds(pl.multiple_of((i // across) * tile_m, tile_m), tile_m)
            to = pl.ds(pl.multiple_of((i % across) * tile_n, tile_n), tile_n)
            x = tok[at, deep]
            g = jnp.dot(x, gate[deep, to], preferred_element_type=jnp.float32)
            u = jnp.dot(x, up[deep, to], preferred_element_type=jnp.float32)
            if not first:
                g = g + gate_acc[at, to]
                u = u + up_acc[at, to]
            if last:
                g = scale[at, :] * g
                u = scale[at, :] * u
                hidden[at, to] = (g / (1.0 + jnp.exp(-g)) * u).astype(jnp.bfloat16)
            else:
                gate_acc[at, to] = g
                up_acc[at, to] = u

    def product(parity, start, out, add=None):
        tile = min(256, half)

        @pl.loop(0, half // tile)
        def _(i):
            at = pl.ds(pl.multiple_of(i * tile, tile), tile)
            src = pl.ds(pl.multiple_of(parity * half + i * tile, tile), tile)
            value = lax.dot_general(
                hidden[src, :], down[pl.ds(pl.multiple_of(start, width), width), :],
                (((1,), (1,)), ((), ())), preferred_element_type=jnp.float32,
            )
            out[at, :] = value.astype(out.dtype)

    def pair_copy(n):
        return pltpu.make_async_remote_copy(
            src_ref=pair_send.at[n], dst_ref=pair_recv.at[n],
            send_sem=p_sent.at[n], recv_sem=p_got.at[n],
            device_id={"tp": sibling}, device_id_type=MESH,
        )

    def z_copy(n, k):
        slot = pl.ds(pl.multiple_of(((z + k) % n_z) * own_tok, own_tok), own_tok)
        return pltpu.make_async_remote_copy(
            src_ref=z_send.at[n, slot, :], dst_ref=z_recv.at[n, k - 1],
            send_sem=z_sent.at[n, k], recv_sem=z_got.at[n, k],
            device_id={"tp": z_peer(k)}, device_id_type=MESH,
        )

    merge = n_z > 2

    def goes_ahead(k):
        return ((z == 0) & (k == n_z - 1)) | ((z == n_z - 1) & (k == 1))

    def ahead_copy(n, k):
        slot = pl.ds(pl.multiple_of(((z + k) % n_z) * own_tok, own_tok), own_tok)
        return pltpu.make_async_remote_copy(
            src_ref=z_send.at[n, slot, :], dst_ref=ahead.at[n], send_sem=a_sent.at[n], recv_sem=a_got.at[n],
            device_id={"tp": (z + 1 if k == n_z - 1 else z - 1) * 2 + core}, device_id_type=MESH,
        )

    def joins(k):
        return ((z == 1) & (k == n_z - 2)) | ((z == n_z - 2) & (k == 2))

    def finish(n):
        pair_copy(n).wait_recv()
        z_send[n] = (pair_own[n % 2] + pair_recv[n].astype(jnp.float32)).astype(jnp.bfloat16)
        if merge:
            for k in (1, n_z - 1):
                @pl.when(goes_ahead(k))
                def _():
                    ahead_copy(n, k).start()
        for k in range(n_z - 1, 0, -1):
            if merge:
                @pl.when(jnp.logical_not(goes_ahead(k) | joins(k)))
                def _():
                    z_copy(n, k).start()
            else:
                z_copy(n, k).start()

    def join(n):
        if merge:
            for k in sorted({2, n_z - 2}):
                @pl.when(joins(k))
                def _():
                    slot = pl.ds(pl.multiple_of(((z + k) % n_z) * own_tok, own_tok), own_tok)
                    pltpu.make_async_remote_copy(
                        src_ref=ahead.at[n], dst_ref=ahead.at[n], send_sem=a_sent.at[n], recv_sem=a_got.at[n],
                        device_id={"tp": sibling}, device_id_type=MESH,
                    ).wait_recv()
                    both = z_send[n, slot, :].astype(jnp.float32) + ahead[n].astype(jnp.float32)
                    z_send[n, slot, :] = both.astype(jnp.bfloat16)
                    z_copy(n, k).start()

    def when_block(mask, p, h):
        return (0,) if mask == 0 else (1, bin(mask).count("1") > 1, arrivals[p, mask], h, p)

    blocks = [(mask, p, h) for mask in range(n_fs) for p in range(dims) for h in range(halves)]
    if pieces == 1:
        chunks = [[(mask, p, h) for p in range(dims) for h in range(halves)] for mask in range(n_fs)]
    else:
        chunks = [[b] for b in sorted(blocks, key=lambda b: when_block(*b))]
    starts = []
    for n, chunk in enumerate(chunks):
        for mask, p, h in chunk:
            need(DOWN, p, h, mask)
        mask, p, h = chunk[0]
        start = flip_all(fs, mask, dims) * rows + p * part + h * width
        starts.append(start)
        product(1 - core, start, pair_send.at[n])
        launch(pair_copy(n))
        if n:
            finish(n - 1)
        if n > 1:
            join(n - 2)
        product(core, start, pair_own.at[n % 2])
    finish(len(chunks) - 1)
    for n in range(max(0, len(chunks) - 2), len(chunks)):
        join(n)

    for n, start in enumerate(starts):
        mine = pl.ds(pl.multiple_of(z * own_tok, own_tok), own_tok)
        to = pl.ds(pl.multiple_of(start, width), width)
        branch = z_send[n, mine, :].astype(jnp.float32)
        for k in range(1, n_z):
            if merge and k in (1, n_z - 1):
                far = ((z == n_z - 1) & (k == n_z - 1)) | ((z == 0) & (k == 1))

                @pl.when(jnp.logical_not(far))
                def _():
                    z_copy(n, k).wait_recv()

                @pl.when(far)
                def _():
                    z_recv[n, k - 1] = jnp.zeros((own_tok, width), jnp.bfloat16)
            else:
                z_copy(n, k).wait_recv()
            branch = branch + z_recv[n, k - 1].astype(jnp.float32)
        mixed[:, to] = (tok_in[:, to].astype(jnp.float32) + 0.5 * branch).astype(jnp.bfloat16)

    for n in range(len(chunks)):
        for k in range(1, n_z):
            if merge and k in (1, n_z - 1):
                @pl.when(goes_ahead(k))
                def _():
                    ahead_copy(n, k).wait_send()

                @pl.when(jnp.logical_not(goes_ahead(k)))
                def _():
                    z_copy(n, k).wait_send()
            else:
                z_copy(n, k).wait_send()
    for copy in started:
        copy.wait_send()


def store(*refs):
    count = len(refs) // 2
    done = refs[-1]
    copies = []
    for n in range(count):
        tall = refs[n].shape[0] // 2
        for h in range(2):
            at = pl.ds(h * tall, tall)
            copies.append(pltpu.make_async_copy(refs[n].at[at, :], refs[count + n].at[at, :], done.at[n, h]))
            copies[-1].start()
    for copy in copies:
        copy.wait()


def body(n_fs, n_tp, tokens, norm_gain, gate_master, up_master, down_master):
    own_tok, depth = tokens.shape
    rows, cols = gate_master.shape
    dims = n_fs.bit_length() - 1
    n_z = n_tp // 2
    half, total = n_z * own_tok, n_tp * own_tok
    part = rows // dims
    halves = part // 128 if part % 128 == 0 else 1
    pieces = dims * halves if part % 128 == 0 else 1
    width, count = rows // pieces, n_fs * pieces
    bf16, f32 = jnp.bfloat16, jnp.float32
    dma = pltpu.SemaphoreType.DMA
    vmem = pl.BlockSpec(memory_space=pltpu.VMEM)
    hbm = pl.BlockSpec(memory_space=pltpu.HBM)
    operands = (tokens, norm_gain[None, :], gate_master, up_master, down_master)
    results = pl.pallas_call(
        functools.partial(kernel, n_fs, n_z, dims, halves, pieces),
        out_shape=(pltpu.VMEM((own_tok, depth), bf16),)
        + tuple(pltpu.VMEM((n_fs * rows, cols), bf16) for _ in range(3)),
        in_specs=[hbm] * 5,
        out_specs=(vmem,) * 4,
        scratch_shapes=[
            pltpu.VMEM((own_tok, depth), bf16),
            pltpu.VMEM((1, rows), f32),
            pltpu.VMEM((rows, 128), f32),
            pltpu.VMEM((3, rows, cols), f32),
            pltpu.VMEM((total, depth), bf16),
            pltpu.VMEM((total, 1), f32),
            pltpu.VMEM((total, cols), f32),
            pltpu.VMEM((total, cols), f32),
            pltpu.VMEM((total, cols), bf16),
            pltpu.VMEM((2, half, width), f32),
            pltpu.VMEM((count, half, width), bf16),
            pltpu.VMEM((count, half, width), bf16),
            pltpu.VMEM((count, half, width), bf16),
            pltpu.VMEM((count, n_z - 1, own_tok, width), bf16),
            pltpu.VMEM((count, own_tok, width), bf16),
            dma((3, dims, halves, n_fs)), dma((3, dims, halves, n_fs)),
            dma((n_z,)), dma((n_z,)),
            dma((n_z,)), dma((n_z,)),
            dma((count,)), dma((count,)),
            dma((count, n_z)), dma((count, n_z)),
            dma((count,)), dma((count,)),
            dma((2 * dims + 3,)),
        ],
        compiler_params=pltpu.CompilerParams(
            collective_id=0, has_side_effects=True, vmem_limit_bytes=40 * 1024 * 1024
        ),
    )(*(pltpu.with_memory_space_constraint(value, pltpu.HBM) for value in operands))
    return pl.pallas_call(
        store,
        out_shape=tuple(jax.ShapeDtypeStruct(result.shape, result.dtype) for result in results),
        in_specs=[vmem] * 4,
        out_specs=(hbm,) * 4,
        scratch_shapes=[dma((4, 2))],
        compiler_params=pltpu.CompilerParams(vmem_limit_bytes=1024 * 1024),
    )(*(pltpu.with_memory_space_constraint(result, pltpu.VMEM) for result in results))


def solution(mesh):
    in_specs = (P(("fs", "tp"), None), P("fs"), P("fs", "tp"), P("fs", "tp"), P("fs", "tp"))
    out_specs = (P(("fs", "tp"), None), P(None, "tp"), P(None, "tp"), P(None, "tp"))
    step = functools.partial(body, mesh.shape["fs"], mesh.shape["tp"])
    return jax.shard_map(step, mesh=mesh, in_specs=in_specs, out_specs=out_specs, check_vma=False)
```

profile of v0, /device:TPU:0, one launch (start us, length us, event | category | flops | bytes accessed | tf_op | source)
XLA Modules:
  0.0 127.7 jit_solution(9190816744762410155)
XLA Ops:
  0.6 122.2 %shard_map.84 = (bf16[128,2048]{1,0:T(8,128)(2,1)S(1)}, bf16[2048,1024]{1,0:T(8,128)(2,1)S(1)}, bf16[2048,1024]{1,0:T(8,128)(2,1)S(1)}, bf16[2048,1024]{1,0:T(8,128)(2,1)S(1)}) custom-call(bf16[128,2048]{1,0:T(8,128)(2,1)} %tok_hbm.1, f32[1,512]{1,0:T(1,128)} %bitcast.1, f32[512,1024]{1,0:T(8,128)} %gate_hbm.1, f32[512,1024]{1,0:T(8,128)} %up_hbm.1, ...), custom_call_target="tpu_custom_call" | custom-call | tf_op jit(solution)/shard_map/pallas_call | solution.py:387
  122.9 4.8 %shard_map.85 = (bf16[128,2048]{1,0:T(8,128)(2,1)}, bf16[2048,1024]{1,0:T(8,128)(2,1)}, bf16[2048,1024]{1,0:T(8,128)(2,1)}, bf16[2048,1024]{1,0:T(8,128)(2,1)}) custom-call(bf16[128,2048]{1,0:T(8,128)(2,1)S(1)} %get-tuple-element.8.refs_0_, bf16[2048,1024]{1,0:T(8,128)(2,1)S(1)} %get-tuple-element.9.refs_1_, ...), custom_call_target="tpu_custom_call" | custom-call | tf_op jit(solution)/shard_map/pallas_call | solution.py:421
where the time goes:
time: 128 us
  Pallas kernels  127 us (99%)
    pallas_call x1, Pallas kernels, body(): pl.pallas_call(functools.partial(kernel, n_fs, n_z, dims, halves, pieces)...  122 us
    pallas_call x1, Pallas kernels, body(): pl.pallas_call(store, out_shape=tuple((jax.ShapeDtypeStruct(result.shape,...  4.84 us

commit v1 on v0

v1 whole, which is shorter than its diff:
```python
import functools
import math

import jax
import jax.numpy as jnp
from jax import lax
from jax.experimental import pallas as pl
from jax.experimental.pallas import tpu as pltpu
from jax.sharding import PartitionSpec as P

MESH = pl.DeviceIdType.MESH
GATE, UP, DOWN = 0, 1, 2


def flip(index, bit):
    return index + bit - 2 * bit * ((index // bit) % 2)


def flip_all(index, mask, dims):
    for dim in range(dims):
        if mask >> dim & 1:
            index = flip(index, 1 << dim)
    return index


def span(bits):
    masks = [0]
    for bit in bits:
        masks += [mask | bit for mask in masks]
    return masks


def plan(n_fs, dims, rows):
    part = rows // dims
    last = n_fs - 1
    if dims != 2 or part % 128 or rows % 256:
        chunks = [([(mask, 0, rows)], [(p, 0, mask) for p in range(dims)], mask) for mask in range(n_fs)]
        return part, part, rows, chunks, last
    chunks = [([(0, at, 256)], [], 0) for at in range(0, rows, 256)]
    for step, owners in enumerate(([(1, 0), (2, 1)], [(2, 0), (1, 1)], [(last, 0), (last, 1)])):
        tall = 64 if step == 2 else 128
        for h in range(part // tall):
            blocks = [(mask, p * part + h * tall, tall) for mask, p in owners]
            chunks.append((blocks, [(p, h, mask) for mask, p in owners], (step, h)))
    return 64, 128, 128, chunks, chunks.index(next(c for c in chunks if c[2] == (1, part // 128 - 1)))


def kernel(
    n_fs, n_z, dims, halves, late_tall, tall_of, width, chunks, first,
    tok_hbm, gain_hbm, gate_hbm, up_hbm, down_hbm,
    mixed, gate, up, down,
    tok_in, gain_row, gain, masters, tok, scale, gate_acc, up_acc, hidden, pair_own, pair_send, pair_recv, z_send, z_pass, z_last,
    w_sent, w_got, t_sent, t_got, s_got, p_sent, p_got, z_sent, z_got, l_got, m_got, loaded,
):
    fs, tp = lax.axis_index("fs"), lax.axis_index("tp")
    z, core = tp // 2, tp % 2
    sibling = z * 2 + 1 - core
    rows, cols = gate_hbm.shape
    part = rows // dims
    own_tok = tok_in.shape[0]
    half = n_z * own_tok
    total = 2 * half
    ready = (gate, up, down)
    every = n_fs - 1

    def cuts(w, mask):
        if w == DOWN:
            return part // (late_tall if mask == every else tall_of)
        return (1, halves)[w]


    loads = {}
    reads = [("gain", gain_hbm, gain_row)]
    for w, master in ((GATE, gate_hbm), (UP, up_hbm)):
        for p in range(dims):
            for i in range(2):
                mine = pl.ds(p * part + i * part // 2, part // 2)
                reads.append(((w, p, i), master.at[mine, :], masters.at[w, mine, :]))
    reads.append(("tok", tok_hbm, tok_in))
    reads.append(("down", down_hbm, masters.at[DOWN]))
    for n, (name, src, dst) in enumerate(reads):
        loads[name] = pltpu.make_async_copy(src, dst, loaded.at[n])

    def z_peer(k):
        return ((z + k) % n_z) * 2 + core

    for name, _, _ in reads[:1 + 2 * dims]:
        loads[name].start()
    barrier = pltpu.get_barrier_semaphore()
    for dim in range(dims):
        pl.semaphore_signal(barrier, 1, device_id={"fs": flip(fs, 1 << dim)}, device_id_type=MESH)
    for k in range(1, n_z):
        pl.semaphore_signal(barrier, 1, device_id={"tp": z_peer(k)}, device_id_type=MESH)
    pl.semaphore_signal(barrier, 1, device_id={"tp": sibling}, device_id_type=MESH)

    loads["gain"].wait()
    for n in range(rows // 128):
        line = gain_row[:, n * 128:(n + 1) * 128]
        gain[n * 128:(n + 1) * 128, :] = jnp.transpose(jnp.broadcast_to(line, (128, 128)))

    def block(w, owner, p, h, mask):
        tall = part // cuts(w, mask)
        start = flip_all(fs, owner, dims) * rows + p * part + h * tall
        return ready[w].at[pl.ds(pl.multiple_of(start, tall), tall), :]

    def order(p):
        return [1 << ((p + s) % dims) for s in range(dims)]

    arrivals = {
        (p, held | order(p)[stage]): stage
        for p in range(dims) for stage in range(dims) for held in span(order(p)[:stage])
    }
    arrived = set()

    place = {}
    for w in (GATE, UP, DOWN):
        for p in range(dims):
            for mask in range(1, n_fs):
                for h in range(cuts(w, mask)):
                    place[w, p, h, mask] = len(place)

    def weight_copy(w, p, h, held, mask, stage):
        return pltpu.make_async_remote_copy(
            src_ref=block(w, held, p, h, mask), dst_ref=block(w, held, p, h, mask),
            send_sem=w_sent.at[w], recv_sem=w_got.at[place[w, p, h, mask]],
            device_id={"fs": flip(fs, order(p)[stage])}, device_id_type=MESH,
        )

    def send(w, p, h, stage, held):
        weight_copy(w, p, h, held, held | order(p)[stage], stage).start()

    def need(w, p, h, mask, hold=False):
        if mask and (w, p, h, mask) not in arrived:
            arrived.add((w, p, h, mask))
            stage = arrivals[p, mask]
            here = block(w, mask, p, h, mask)
            pltpu.make_async_remote_copy(
                src_ref=here, dst_ref=here, send_sem=w_sent.at[w], recv_sem=w_got.at[place[w, p, h, mask]],
                device_id={"fs": flip(fs, order(p)[stage])}, device_id_type=MESH,
            ).wait_recv()
            if not hold:
                forward(w, p, h, mask)

    def forward(w, p, h, mask):
        for later in range(arrivals[p, mask] + 1, dims):
            finer = cuts(w, mask | order(p)[later]) // cuts(w, mask)
            for piece in range(h * finer, (h + 1) * finer):
                send(w, p, piece, later, mask)

    def relays(ws):
        for stage in range(dims - 1):
            for w in ws:
                for p in range(dims):
                    for held in span(order(p)[:stage]):
                        for h in range(cuts(w, held | order(p)[stage])):
                            need(w, p, h, held | order(p)[stage])

    def prepare(w, top, tall):
        mine = slice(top, top + tall)
        value = masters[w, mine, :]
        if w != DOWN:
            value = gain[mine, 0:1] * value
        ready[w][pl.ds(pl.multiple_of(fs * rows + top, tall), tall), :] = value.astype(jnp.bfloat16)

    short = part // 2
    for p in range(dims):
        for i in range(2):
            loads[GATE, p, i].wait()
            prepare(GATE, p * part + i * short, short)
            if p == 0 and i == 0:
                with jax.named_scope("barrier"):
                    pl.semaphore_wait(barrier, dims + n_z)
            at = gate.at[pl.ds(pl.multiple_of(fs * rows + p * part + i * short, short), short), :]
            pltpu.make_async_remote_copy(
                src_ref=at, dst_ref=at, send_sem=w_sent.at[GATE], recv_sem=w_got.at[place[GATE, p, 0, order(p)[0]]],
                device_id={"fs": flip(fs, order(p)[0])}, device_id_type=MESH,
            ).start()
    for name, _, _ in reads[1 + 2 * dims:]:
        loads[name].start()
    for p in range(dims):
        for i in range(2):
            loads[UP, p, i].wait()
        prepare(UP, p * part, part)
        for h in range(cuts(UP, 0)):
            send(UP, p, h, 0, 0)

    def tok_rows(c, chip):
        start = (c * n_z + chip) * own_tok
        return tok.at[pl.ds(pl.multiple_of(start, own_tok), own_tok), :]

    def tok_z(k):
        return pltpu.make_async_remote_copy(
            src_ref=tok_in, dst_ref=tok_rows(core, z), send_sem=t_sent.at[0], recv_sem=t_got.at[k],
            device_id={"tp": z_peer(k)}, device_id_type=MESH,
        )

    def tok_sibling(k, src, slot):
        return pltpu.make_async_remote_copy(
            src_ref=src, dst_ref=slot, send_sem=t_sent.at[0], recv_sem=s_got.at[k],
            device_id={"tp": sibling}, device_id_type=MESH,
        )

    loads["tok"].wait()
    for k in range(1, n_z):
        tok_z(k).start()
    tok_sibling(0, tok_in, tok_rows(core, z)).start()
    for w in (GATE, UP):
        for p in range(dims):
            for stage in range(1, dims):
                for h in range(cuts(w, 0)):
                    send(w, p, h, stage, 0)
    tok_rows(core, z)[...] = tok_in[...]
    loads["down"].wait()
    for p in range(dims):
        prepare(DOWN, p * part, part)

    @pl.when(z == 0)
    def _():
        z_last[0] = jnp.zeros(z_last.shape[1:], jnp.bfloat16)

    @pl.when(z == n_z - 1)
    def _():
        z_last[1] = jnp.zeros(z_last.shape[1:], jnp.bfloat16)

    with jax.named_scope("relays"):
        relays((GATE, UP))

    def send_down(turn, stages):
        @pl.when(core == turn)
        def _():
            for stage in stages:
                for h in range(max(cuts(DOWN, order(p)[stage]) for p in range(dims))):
                    for p in range(dims):
                        send(DOWN, p, h, stage, 0)

    split = dims == 2 and first > 4
    send_down(0, range(1) if split else range(dims))

    for k in range(1, n_z):
        slot = tok_rows(core, (z + n_z - k) % n_z)
        with jax.named_scope(f"tokwait{k}"):
            pltpu.make_async_remote_copy(
                src_ref=slot, dst_ref=slot, send_sem=t_sent.at[0], recv_sem=t_got.at[k],
                device_id={"tp": z_peer(k)}, device_id_type=MESH,
            ).wait_recv()
        tok_sibling(k, slot, slot).start()
    for k in range(n_z):
        slot = tok_rows(1 - core, (z + n_z - k) % n_z)
        with jax.named_scope(f"tokpair{k}"):
            tok_sibling(k, slot, slot).wait_recv()

    tile_m, tile_n = min(256, half), min(512, cols)
    across = cols // tile_n
    tile_s = min(64, total)
    f32 = jnp.float32

    @pl.loop(0, total // tile_s)
    def _(i):
        at = pl.ds(pl.multiple_of(i * tile_s, tile_s), tile_s)
        wide = tok[at, :].astype(f32)
        scale[at, :] = lax.rsqrt(jnp.mean(wide * wide, axis=1, keepdims=True) + 1e-06)

    def tiles(count, first, run):
        @pl.loop(0, (count // tile_m) * across)
        def _(i):
            at = pl.ds(pl.multiple_of(first + (i // across) * tile_m, tile_m), tile_m)
            run(at, pl.ds(pl.multiple_of((i % across) * tile_n, tile_n), tile_n))

    def deep(mask):
        return pl.ds(pl.multiple_of(flip_all(fs, mask, dims) * rows, rows), rows)

    def dot(x, w):
        return jnp.dot(x, w, preferred_element_type=f32)

    def piece_dot(at, to, h):
        if halves == 1:
            return dot(tok[at, deep(every)], up[deep(every), to])
        tall = part // halves
        owner = flip_all(fs, every, dims) * rows
        spots = [pl.ds(pl.multiple_of(owner + p * part + h * tall, tall), tall) for p in range(dims)]
        x = jnp.concatenate([tok[at, spot] for spot in spots], axis=1)
        return dot(x, jnp.concatenate([up[spot, to] for spot in spots], axis=0))

    for mask in range(every):
        for w in (GATE, UP):
            for p in range(dims):
                for h in range(cuts(w, mask)):
                    with jax.named_scope(f"early_need{mask}{w}{p}{h}"):
                        need(w, p, h, mask)

    def early(at, to):
        g, u = dot(tok[at, deep(0)], gate[deep(0), to]), dot(tok[at, deep(0)], up[deep(0), to])
        for mask in range(1, every):
            g = g + dot(tok[at, deep(mask)], gate[deep(mask), to])
            u = u + dot(tok[at, deep(mask)], up[deep(mask), to])
        gate_acc[at, to] = g
        up_acc[at, to] = u

    with jax.named_scope("early"):
        tiles(total, 0, early)

    for p in range(dims):
        with jax.named_scope(f"gate_need{p}"):
            need(GATE, p, 0, every)

    def gate_end(at, to):
        g = scale[at, :] * (gate_acc[at, to] + dot(tok[at, deep(every)], gate[deep(every), to]))
        gate_acc[at, to] = scale[at, :] * (g / (1.0 + jnp.exp(-g)))

    with jax.named_scope("gate_end"):
        tiles(total, 0, gate_end)

    for h in range(cuts(UP, every) - 1):
        for p in range(dims):
            with jax.named_scope(f"up_need{h}{p}"):
                need(UP, p, h, every)

        def up_more(at, to):
            up_acc[at, to] = up_acc[at, to] + piece_dot(at, to, h)

        with jax.named_scope(f"up_more{h}"):
            tiles(total, 0, up_more)

    for p in range(dims):
        with jax.named_scope(f"up_need{cuts(UP, every) - 1}{p}"):
            need(UP, p, cuts(UP, every) - 1, every)

    send_down(1, range(dims))

    def up_end(at, to):
        u = up_acc[at, to] + piece_dot(at, to, cuts(UP, every) - 1)
        hidden[at, to] = (gate_acc[at, to] * u).astype(jnp.bfloat16)

    units = [sum(tall for _, _, tall in blocks) // width for blocks, _, _ in chunks]
    bounds = [sum(units[:n]) for n in range(len(units) + 1)]
    count = len(chunks)

    def slot_rows(d):
        return pl.ds(pl.multiple_of(d * own_tok, own_tok), own_tok)

    def product(n, parity, out, slot=None):
        tile = own_tok if slot is not None else min(256, half)
        spots = []
        for mask, top, tall in chunks[n][0]:
            start = flip_all(fs, mask, dims) * rows + top
            spots.append(pl.ds(pl.multiple_of(start, math.gcd(tall, top) if top else tall), tall))

        def run(i):
            at = pl.ds(pl.multiple_of(i * tile, tile), tile)
            src = pl.ds(pl.multiple_of(parity * half + i * tile, tile), tile)
            w = [down[spot, :] for spot in spots]
            value = lax.dot_general(
                hidden[src, :], w[0] if len(w) == 1 else jnp.concatenate(w, axis=0),
                (((1,), (1,)), ((), ())), preferred_element_type=f32,
            )
            for unit in range(units[n]):
                out(unit)[at, :] = value[:, unit * width:(unit + 1) * width].astype(out(unit).dtype)

        if slot is not None:
            run(slot)
        else:
            pl.loop(0, half // tile)(run)

    def pair_copy(n, i=None, slot=None):
        mine = pl.ds(bounds[n], units[n])
        at = (mine,) if slot is None else (mine, slot_rows(slot))
        return pltpu.make_async_remote_copy(
            src_ref=pair_send.at[at], dst_ref=pair_recv.at[at],
            send_sem=p_sent.at[0], recv_sem=p_got.at[n if i is None else count + i],
            device_id={"tp": sibling}, device_id_type=MESH,
        )

    def passing(side, hops):
        return hops - 1 if side > 0 else n_z - 1 - hops

    deal = units[0]
    meets = range(first, count - 1 if n_z > 3 else first)

    def chain_copy(n, side, hops):
        mine = pl.ds(n * deal, deal)
        if hops == 1:
            dst, got = z_last.at[(1 - side) // 2, mine], l_got.at[(1 - side) // 2]
        else:
            dst, got = z_pass.at[mine, passing(side, hops - 1)], z_got.at[n, passing(side, hops - 1)]
        to = jnp.clip(z + side, 0, n_z - 1)
        return pltpu.make_async_remote_copy(
            src_ref=z_send.at[mine, slot_rows(jnp.clip(z + side * hops, 0, n_z - 1)), :], dst_ref=dst,
            send_sem=z_sent.at[0], recv_sem=got,
            device_id={"tp": to * 2 + core}, device_id_type=MESH,
        )

    def straight_copy(n, k):
        mine = pl.ds(bounds[n], units[n])
        return pltpu.make_async_remote_copy(
            src_ref=z_send.at[mine, slot_rows((z + k) % n_z), :], dst_ref=z_pass.at[mine, k - 1],
            send_sem=z_sent.at[0], recv_sem=z_got.at[n, k - 1],
            device_id={"tp": z_peer(k)}, device_id_type=MESH,
        )

    def meet_copy(n, to):
        mine = pl.ds(bounds[n], units[n])
        return pltpu.make_async_remote_copy(
            src_ref=z_send.at[mine, slot_rows(to), :], dst_ref=z_last.at[0, mine],
            send_sem=z_sent.at[0], recv_sem=m_got.at[n - first],
            device_id={"tp": jnp.where(z == 0, 1, n_z - 2) * 2 + core}, device_id_type=MESH,
        )

    def meet(n):
        for at, to in ((1, n_z - 1), (n_z - 2, 0)):
            @pl.when(z == at)
            def _():
                meet_copy(n, to).wait_recv()
                for unit in range(bounds[n], bounds[n + 1]):
                    rest = slice(to * own_tok, (to + 1) * own_tok)
                    both = z_send[unit, rest, :].astype(f32) + z_last[0, unit].astype(f32)
                    z_send[unit, rest, :] = both.astype(jnp.bfloat16)
                straight_copy(n, (to - at) % n_z).start()

    def at_ends(run):
        for side, end in ((1, 0), (-1, n_z - 1)):
            @pl.when(z == end)
            def _():
                run(side)

    def finish(n):
        pair_copy(n).wait_recv()
        for unit in range(units[n]):
            at = bounds[n] + unit
            z_send[at] = (pair_own[n % 2, unit] + pair_recv[at].astype(f32)).astype(jnp.bfloat16)
        if n in meets:
            for k in range(n_z - 1, 0, -1):
                hop = jnp.where(z < n_z // 2, k, n_z - k)
                to = (z + hop) % n_z
                across_all = ((z == 0) & (to == n_z - 1)) | ((z == n_z - 1) & (to == 0))
                waits = ((z == 1) & (to == n_z - 1)) | ((z == n_z - 2) & (to == 0))

                @pl.when(across_all)
                def _():
                    meet_copy(n, to).start()

                @pl.when(jnp.logical_not(across_all | waits))
                def _():
                    straight_copy(n, hop).start()
        elif n >= first:
            for k in range(n_z - 1, 0, -1):
                straight_copy(n, jnp.where(z < n_z // 2, k, n_z - k)).start()
        else:
            at_ends(lambda side: [chain_copy(n, side, hops).start() for hops in range(n_z - 1, 0, -1)])

    def pass_on(n, depth, side):
        mine = pl.ds(n * deal, deal)
        for hops in range(n_z - 2, 0, -1):
            @pl.when(depth + hops < n_z)
            def _():
                at = passing(side, hops)
                pltpu.make_async_remote_copy(
                    src_ref=z_pass.at[mine, at], dst_ref=z_pass.at[mine, at],
                    send_sem=z_sent.at[0], recv_sem=z_got.at[n, at],
                    device_id={"tp": sibling}, device_id_type=MESH,
                ).wait_recv()
                to = slot_rows(jnp.clip(z + side * hops, 0, n_z - 1))
                both = z_send[mine, to, :].astype(f32) + z_pass[mine, at].astype(f32)
                z_send[mine, to, :] = both.astype(jnp.bfloat16)
                chain_copy(n, side, hops).start()

    def relay(t):
        for side in (1, -1):
            depth = z if side > 0 else n_z - 1 - z
            inner = (depth > 0) & (depth < n_z - 1)
            for late in (1, 0):
                n = t - depth - late
                slow = (n < 2) | ((n == first - 1) & (depth > 1))
                turn = inner & (n >= 0) & (n < first) & (slow if late else jnp.logical_not(slow))

                @pl.when(turn)
                def _():
                    pass_on(n, depth, side)

    def open_up():
        slots = [jnp.where(z < n_z // 2, n_z - 1 - i, i) for i in range(n_z)]

        def half_of(parity, slot):
            first_row = parity * half + slot * own_tok
            at = pl.ds(pl.multiple_of(first_row, own_tok), own_tok)
            for j in range(across):
                up_end(at, slice(j * tile_n, (j + 1) * tile_n))

        def away(i):
            half_of(1 - core, slots[i])
            product(0, 1 - core, lambda unit: pair_send.at[unit], slots[i])
            pair_copy(0, i, slots[i]).start()

        def close(i):
            half_of(core, slots[i])
            product(0, core, lambda unit: pair_own.at[0, unit], slots[i])
            pair_copy(0, i, slots[i]).wait_recv()
            here = slot_rows(slots[i])
            for unit in range(deal):
                own = pair_own[0, unit, here, :] + pair_recv[unit, here, :].astype(f32)
                z_send[unit, here, :] = own.astype(jnp.bfloat16)
            if i < n_z - 1:
                at_ends(lambda side: chain_copy(0, side, n_z - 1 - i).start())

        for i in range(n_z):
            with jax.named_scope(f"away{i}"):
                away(i)
            if i:
                with jax.named_scope(f"close{i - 1}"):
                    close(i - 1)
        with jax.named_scope(f"close{n_z - 1}"):
            close(n_z - 1)

    with jax.named_scope("open"):
        open_up()
    finished = 1
    for n, (blocks, needs, wave) in enumerate(chunks):
        if n == 0:
            continue
        if split and n == 3:
            send_down(0, range(1, dims))
        for p, h, mask in needs:
            with jax.named_scope(f"d{n}_need"):
                need(DOWN, p, h, mask, hold=split and n in (2, 3))
        if split and n == 3:
            for p, h, mask in chunks[2][1] + chunks[3][1]:
                forward(DOWN, p, h, mask)
        with jax.named_scope(f"d{n}_prodA"):
            product(n, 1 - core, lambda unit: pair_send.at[bounds[n] + unit])
            pair_copy(n).start()
        if n >= first:
            with jax.named_scope(f"d{n}_relay"):
                relay(n)
                if n - 2 in meets:
                    meet(n - 2)
        with jax.named_scope(f"d{n}_finish"):
            if finished < n:
                finish(n - 1)
                finished = n
        with jax.named_scope(f"d{n}_prodB"):
            product(n, core, lambda unit: pair_own.at[n % 2, unit])
        if n + 1 == count or chunks[n + 1][2] != wave:
            with jax.named_scope(f"d{n}_finish"):
                finish(n)
                finished = n + 1
        if n < first:
            with jax.named_scope(f"d{n}_relay"):
                relay(n)
    with jax.named_scope("lastrelay"):
        for t in range(count, first + n_z):
            relay(t)
        for n in meets:
            if n + 2 >= count:
                meet(n)

    mine = slot_rows(z)

    def total_of(unit):
        branch = z_send[unit, mine, :].astype(f32)
        if unit < bounds[first]:
            return branch + z_last[0, unit].astype(f32) + z_last[1, unit].astype(f32)
        for k in range(n_z - 1):
            branch = branch + z_pass[unit, k].astype(f32)
        return branch

    def settle(mask, top, parts):
        start = flip_all(fs, mask, dims) * rows + top
        to = pl.ds(pl.multiple_of(start, width), width)
        branch = jnp.concatenate(parts, axis=1) if len(parts) > 1 else parts[0]
        mixed[:, to] = (tok_in[:, to].astype(f32) + 0.5 * branch).astype(jnp.bfloat16)

    with jax.named_scope("lastwait"):
        spread = pl.ds(0, bounds[first])
        for side, end in ((0, 0), (1, n_z - 1)):
            @pl.when(z != end)
            def _():
                pltpu.make_async_remote_copy(
                    src_ref=z_last.at[side, spread], dst_ref=z_last.at[side, spread],
                    send_sem=z_sent.at[0], recv_sem=l_got.at[side],
                    device_id={"tp": sibling}, device_id_type=MESH,
                ).wait_recv()
    open_parts = {}
    for n, (blocks, _, _) in enumerate(chunks):
        with jax.named_scope(f"last{n}"):
            if n >= first:
                for k in range(1, n_z):
                    absent = ((z == n_z - 1) & (k == n_z - 1)) | ((z == 0) & (k == 1))
                    if n not in meets:
                        straight_copy(n, k).wait_recv()
                    elif k in (1, n_z - 1):
                        @pl.when(jnp.logical_not(absent))
                        def _():
                            straight_copy(n, k).wait_recv()

                        @pl.when(absent)
                        def _():
                            spread = pl.ds(bounds[n], units[n])
                            z_pass[spread, k - 1] = jnp.zeros((units[n], own_tok, width), jnp.bfloat16)
                    else:
                        straight_copy(n, k).wait_recv()
            sums = [total_of(unit) for unit in range(bounds[n], bounds[n + 1])]
            lane = 0
            for mask, top, tall in blocks:
                if tall < width:
                    key = (mask, top // width * width)
                    open_parts.setdefault(key, []).append(sums[0][:, lane:lane + tall])
                    lane += tall
                    if sum(piece.shape[1] for piece in open_parts[key]) == width:
                        settle(mask, key[1], open_parts.pop(key))
                    continue
                for at in range(0, tall, width):
                    settle(mask, top + at, [sums[lane // width]])
                    lane += width

    def sent(ref, sem):
        pltpu.make_async_remote_copy(
            src_ref=ref, dst_ref=ref, send_sem=sem, recv_sem=sem,
            device_id={"tp": sibling}, device_id_type=MESH,
        ).wait_send()

    for w in range(3):
        sent(ready[w].at[pl.ds(0, every * rows), :], w_sent.at[w])
    sent(tok.at[pl.ds(0, (2 * n_z - 1) * own_tok), :], t_sent.at[0])
    sent(pair_send, p_sent.at[0])
    sent(z_pass, z_sent.at[0])


def store(*refs):
    count = len(refs) // 2
    done = refs[-1]
    copies = []
    for n in range(count):
        tall = refs[n].shape[0] // 2
        for h in range(2):
            at = pl.ds(h * tall, tall)
            copies.append(pltpu.make_async_copy(refs[n].at[at, :], refs[count + n].at[at, :], done.at[n, h]))
            copies[-1].start()
    for copy in copies:
        copy.wait()


def body(n_fs, n_tp, tokens, norm_gain, gate_master, up_master, down_master):
    own_tok, depth = tokens.shape
    rows, cols = gate_master.shape
    dims = n_fs.bit_length() - 1
    n_z = n_tp // 2
    half, total = n_z * own_tok, n_tp * own_tok
    part = rows // dims
    halves = part // 128 if part % 128 == 0 else 1
    late_tall, tall_of, width, chunks, first = plan(n_fs, dims, rows)
    count, deal = n_fs * rows // width, sum(tall for _, _, tall in chunks[0][0]) // width
    steps = len(chunks)
    pieces = dims * ((n_fs - 1) * (1 + halves) + (n_fs - 2) * (part // tall_of) + part // late_tall)
    bf16, f32 = jnp.bfloat16, jnp.float32
    dma = pltpu.SemaphoreType.DMA
    vmem = pl.BlockSpec(memory_space=pltpu.VMEM)
    hbm = pl.BlockSpec(memory_space=pltpu.HBM)
    operands = (tokens, norm_gain[None, :], gate_master, up_master, down_master)
    results = pl.pallas_call(
        functools.partial(kernel, n_fs, n_z, dims, halves, late_tall, tall_of, width, chunks, first),
        out_shape=(pltpu.VMEM((own_tok, depth), bf16),)
        + tuple(pltpu.VMEM((n_fs * rows, cols), bf16) for _ in range(3)),
        in_specs=[hbm] * 5,
        out_specs=(vmem,) * 4,
        scratch_shapes=[
            pltpu.VMEM((own_tok, depth), bf16),
            pltpu.VMEM((1, rows), f32),
            pltpu.VMEM((rows, 128), f32),
            pltpu.VMEM((3, rows, cols), f32),
            pltpu.VMEM((total, depth), bf16),
            pltpu.VMEM((total, 1), f32),
            pltpu.VMEM((total, cols), f32),
            pltpu.VMEM((total, cols), f32),
            pltpu.VMEM((total, cols), bf16),
            pltpu.VMEM((2, deal, half, width), f32),
            pltpu.VMEM((count, half, width), bf16),
            pltpu.VMEM((count, half, width), bf16),
            pltpu.VMEM((count, half, width), bf16),
            pltpu.VMEM((count, n_z - 1, own_tok, width), bf16),
            pltpu.VMEM((2, count, own_tok, width), bf16),
            dma((3,)), dma((pieces,)),
            dma((1,)), dma((n_z,)), dma((n_z,)),
            dma((1,)), dma((steps + n_z,)),
            dma((1,)), dma((steps, n_z - 1)), dma((2,)), dma((steps - first,)),
            dma((4 * dims + 3,)),
        ],
        compiler_params=pltpu.CompilerParams(
            collective_id=0, has_side_effects=True, vmem_limit_bytes=40 * 1024 * 1024
        ),
    )(*(pltpu.with_memory_space_constraint(value, pltpu.HBM) for value in operands))
    return pl.pallas_call(
        store,
        out_shape=tuple(jax.ShapeDtypeStruct(result.shape, result.dtype) for result in results),
        in_specs=[vmem] * 4,
        out_specs=(hbm,) * 4,
        scratch_shapes=[dma((4, 2))],
        compiler_params=pltpu.CompilerParams(vmem_limit_bytes=1024 * 1024),
    )(*(pltpu.with_memory_space_constraint(result, pltpu.VMEM) for result in results))


def solution(mesh):
    in_specs = (P(("fs", "tp"), None), P("fs"), P("fs", "tp"), P("fs", "tp"), P("fs", "tp"))
    out_specs = (P(("fs", "tp"), None), P(None, "tp"), P(None, "tp"), P(None, "tp"))
    step = functools.partial(body, mesh.shape["fs"], mesh.shape["tp"])
    return jax.shard_map(step, mesh=mesh, in_specs=in_specs, out_specs=out_specs, check_vma=False)
```

time: 128 us -> 123 us (0.961)
  Pallas kernels: 127 us -> 122 us
    pallas_call x1, Pallas kernels: 122 us -> 117 us  [body(): pl.pallas_call(functools.partial(kernel, n_fs, n_z, dims, halves, late_ta...]
where the time goes in v1:
time: 123 us
  Pallas kernels  122 us (99%)
    pallas_call x1, Pallas kernels, body(): pl.pallas_call(functools.partial(kernel, n_fs, n_z, dims, halves, late_ta...  117 us
    pallas_call x1, Pallas kernels, body(): pl.pallas_call(store, out_shape=tuple((jax.ShapeDtypeStruct(result.shape,...  4.84 us

profile of v1, /device:TPU:0, one launch (start us, length us, event | category | flops | bytes accessed | tf_op | source)
XLA Modules:
  0.0 122.9 jit_solution(4516633197661495622)
XLA Ops:
  0.6 117.4 %shard_map.84 = (bf16[128,2048]{1,0:T(8,128)(2,1)S(1)}, bf16[2048,1024]{1,0:T(8,128)(2,1)S(1)}, bf16[2048,1024]{1,0:T(8,128)(2,1)S(1)}, bf16[2048,1024]{1,0:T(8,128)(2,1)S(1)}) custom-call(bf16[128,2048]{1,0:T(8,128)(2,1)} %tok_hbm.1, f32[1,512]{1,0:T(1,128)} %bitcast.1, f32[512,1024]{1,0:T(8,128)} %gate_hbm.1, f32[512,1024]{1,0:T(8,128)} %up_hbm.1, ...), custom_call_target="tpu_custom_call" | custom-call | tf_op jit(solution)/shard_map/pallas_call | solution.py:658
  118.0 4.8 %shard_map.85 = (bf16[128,2048]{1,0:T(8,128)(2,1)}, bf16[2048,1024]{1,0:T(8,128)(2,1)}, bf16[2048,1024]{1,0:T(8,128)(2,1)}, bf16[2048,1024]{1,0:T(8,128)(2,1)}) custom-call(bf16[128,2048]{1,0:T(8,128)(2,1)S(1)} %get-tuple-element.8.refs_0_, bf16[2048,1024]{1,0:T(8,128)(2,1)S(1)} %get-tuple-element.9.refs_1_, ...), custom_call_target="tpu_custom_call" | custom-call | tf_op jit(solution)/shard_map/pallas_call | solution.py:690

commit v2 on v1

--- a/solution.py
+++ b/solution.py
@@ -35,22 +35,23 @@
     last = n_fs - 1
     if dims != 2 or part % 128 or rows % 256:
         chunks = [([(mask, 0, rows)], [(p, 0, mask) for p in range(dims)], mask) for mask in range(n_fs)]
-        return part, part, rows, chunks, last
+        return [part], [part], rows, chunks, last
+    late, other = [64] * (part // 64), [128] * (part // 128)
     chunks = [([(0, at, 256)], [], 0) for at in range(0, rows, 256)]
     for step, owners in enumerate(([(1, 0), (2, 1)], [(2, 0), (1, 1)], [(last, 0), (last, 1)])):
-        tall = 64 if step == 2 else 128
-        for h in range(part // tall):
-            blocks = [(mask, p * part + h * tall, tall) for mask, p in owners]
+        heights = late if step == 2 else other
+        for h, tall in enumerate(heights):
+            blocks = [(mask, p * part + sum(heights[:h]), tall) for mask, p in owners]
             chunks.append((blocks, [(p, h, mask) for mask, p in owners], (step, h)))
-    return 64, 128, 128, chunks, chunks.index(next(c for c in chunks if c[2] == (1, part // 128 - 1)))
+    return late, other, 128, chunks, next(n for n, chunk in enumerate(chunks) if chunk[2] == (1, len(other) - 1))
 
 
 def kernel(
-    n_fs, n_z, dims, halves, late_tall, tall_of, width, chunks, first,
+    n_fs, n_z, dims, halves, late, other, width, chunks, first,
     tok_hbm, gain_hbm, gate_hbm, up_hbm, down_hbm,
     mixed, gate, up, down,
     tok_in, gain_row, gain, masters, tok, scale, gate_acc, up_acc, hidden, pair_own, pair_send, pair_recv, z_send, z_pass, z_last,
-    w_sent, w_got, t_sent, t_got, s_got, p_sent, p_got, z_sent, z_got, l_got, m_got, loaded,
+    w_sent, w_got, t_sent, t_got, s_got, p_sent, p_got, z_sent, z_got, l_got, f_got, m_got, loaded,
 ):
     fs, tp = lax.axis_index("fs"), lax.axis_index("tp")
     z, core = tp // 2, tp % 2
@@ -63,11 +64,14 @@
     ready = (gate, up, down)
     every = n_fs - 1
 
+    def heights(w, mask):
+        if w == DOWN:
+            return late if mask == every else other
+        many = (1, halves)[w]
+        return [part // many] * many
+
     def cuts(w, mask):
-        if w == DOWN:
-            return part // (late_tall if mask == every else tall_of)
-        return (1, halves)[w]
-
+        return len(heights(w, mask))
 
     loads = {}
     reads = [("gain", gain_hbm, gain_row)]
@@ -99,8 +103,8 @@
         gain[n * 128:(n + 1) * 128, :] = jnp.transpose(jnp.broadcast_to(line, (128, 128)))
 
     def block(w, owner, p, h, mask):
-        tall = part // cuts(w, mask)
-        start = flip_all(fs, owner, dims) * rows + p * part + h * tall
+        tall, top = heights(w, mask)[h], sum(heights(w, mask)[:h])
+        start = flip_all(fs, owner, dims) * rows + p * part + top
         return ready[w].at[pl.ds(pl.multiple_of(start, tall), tall), :]
 
     def order(p):
@@ -112,17 +116,25 @@
     }
     arrived = set()
 
+    def together(w, p, h, mask):
+        if dims != 2:
+            return [(p, mask)]
+        return sorted([(p, mask), (1 - p, mask if mask == every else every - mask)])
+
     place = {}
     for w in (GATE, UP, DOWN):
         for p in range(dims):
             for mask in range(1, n_fs):
                 for h in range(cuts(w, mask)):
-                    place[w, p, h, mask] = len(place)
+                    place.setdefault((w, h, *together(w, p, h, mask)), len(place))
+
+    def got(w, p, h, mask):
+        return w_got.at[place[(w, h, *together(w, p, h, mask))]]
 
     def weight_copy(w, p, h, held, mask, stage):
         return pltpu.make_async_remote_copy(
             src_ref=block(w, held, p, h, mask), dst_ref=block(w, held, p, h, mask),
-            send_sem=w_sent.at[w], recv_sem=w_got.at[place[w, p, h, mask]],
+            send_sem=w_sent.at[w], recv_sem=got(w, p, h, mask),
             device_id={"fs": flip(fs, order(p)[stage])}, device_id_type=MESH,
         )
 
@@ -131,21 +143,24 @@
 
     def need(w, p, h, mask, hold=False):
         if mask and (w, p, h, mask) not in arrived:
-            arrived.add((w, p, h, mask))
-            stage = arrivals[p, mask]
-            here = block(w, mask, p, h, mask)
+            pair = together(w, p, h, mask)
+            tall = heights(w, mask)[h] * len(pair)
+            here = ready[w].at[pl.ds(0, tall), :] if len(pair) > 1 else block(w, mask, p, h, mask)
             pltpu.make_async_remote_copy(
-                src_ref=here, dst_ref=here, send_sem=w_sent.at[w], recv_sem=w_got.at[place[w, p, h, mask]],
-                device_id={"fs": flip(fs, order(p)[stage])}, device_id_type=MESH,
+                src_ref=here, dst_ref=here, send_sem=w_sent.at[w], recv_sem=got(w, p, h, mask),
+                device_id={"fs": flip(fs, 1)}, device_id_type=MESH,
             ).wait_recv()
-            if not hold:
-                forward(w, p, h, mask)
+            for p, mask in pair:
+                arrived.add((w, p, h, mask))
+                if not hold:
+                    forward(w, p, h, mask)
 
     def forward(w, p, h, mask):
         for later in range(arrivals[p, mask] + 1, dims):
-            finer = cuts(w, mask | order(p)[later]) // cuts(w, mask)
-            for piece in range(h * finer, (h + 1) * finer):
-                send(w, p, piece, later, mask)
+            top, finer = sum(heights(w, mask)[:h]), heights(w, mask | order(p)[later])
+            for piece in range(len(finer)):
+                if top <= sum(finer[:piece]) < top + heights(w, mask)[h]:
+                    send(w, p, piece, later, mask)
 
     def relays(ws):
         for stage in range(dims - 1):
@@ -172,7 +187,7 @@
                     pl.semaphore_wait(barrier, dims + n_z)
             at = gate.at[pl.ds(pl.multiple_of(fs * rows + p * part + i * short, short), short), :]
             pltpu.make_async_remote_copy(
-                src_ref=at, dst_ref=at, send_sem=w_sent.at[GATE], recv_sem=w_got.at[place[GATE, p, 0, order(p)[0]]],
+                src_ref=at, dst_ref=at, send_sem=w_sent.at[GATE], recv_sem=got(GATE, p, 0, order(p)[0]),
                 device_id={"fs": flip(fs, order(p)[0])}, device_id_type=MESH,
             ).start()
     for name, _, _ in reads[1 + 2 * dims:]:
@@ -190,20 +205,20 @@
 
     def tok_z(k):
         return pltpu.make_async_remote_copy(
-            src_ref=tok_in, dst_ref=tok_rows(core, z), send_sem=t_sent.at[0], recv_sem=t_got.at[k],
+            src_ref=tok_in, dst_ref=tok_rows(core, z), send_sem=t_sent.at[0], recv_sem=t_got.at[k - 1],
             device_id={"tp": z_peer(k)}, device_id_type=MESH,
         )
 
-    def tok_sibling(k, src, slot):
+    def tok_sibling(src, slot):
         return pltpu.make_async_remote_copy(
-            src_ref=src, dst_ref=slot, send_sem=t_sent.at[0], recv_sem=s_got.at[k],
+            src_ref=src, dst_ref=slot, send_sem=t_sent.at[0], recv_sem=s_got.at[0],
             device_id={"tp": sibling}, device_id_type=MESH,
         )
 
     loads["tok"].wait()
     for k in range(1, n_z):
         tok_z(k).start()
-    tok_sibling(0, tok_in, tok_rows(core, z)).start()
+    tok_sibling(tok_in, tok_rows(core, z)).start()
     for w in (GATE, UP):
         for p in range(dims):
             for stage in range(1, dims):
@@ -240,14 +255,16 @@
         slot = tok_rows(core, (z + n_z - k) % n_z)
         with jax.named_scope(f"tokwait{k}"):
             pltpu.make_async_remote_copy(
-                src_ref=slot, dst_ref=slot, send_sem=t_sent.at[0], recv_sem=t_got.at[k],
+                src_ref=slot, dst_ref=slot, send_sem=t_sent.at[0], recv_sem=t_got.at[k - 1],
                 device_id={"tp": z_peer(k)}, device_id_type=MESH,
             ).wait_recv()
-        tok_sibling(k, slot, slot).start()
-    for k in range(n_z):
-        slot = tok_rows(1 - core, (z + n_z - k) % n_z)
-        with jax.named_scope(f"tokpair{k}"):
-            tok_sibling(k, slot, slot).wait_recv()
+        tok_sibling(slot, slot).start()
+    rest = tok.at[pl.ds(pl.multiple_of((1 - core) * half, half), half), :]
+    with jax.named_scope("tokpair"):
+        pltpu.make_async_remote_copy(
+            src_ref=rest, dst_ref=rest, send_sem=t_sent.at[0], recv_sem=s_got.at[0],
+            device_id={"tp": sibling}, device_id_type=MESH,
+        ).wait_recv()
 
     tile_m, tile_n = min(256, half), min(512, cols)
     across = cols // tile_n
@@ -331,7 +348,9 @@
         u = up_acc[at, to] + piece_dot(at, to, cuts(UP, every) - 1)
         hidden[at, to] = (gate_acc[at, to] * u).astype(jnp.bfloat16)
 
-    units = [sum(tall for _, _, tall in blocks) // width for blocks, _, _ in chunks]
+    spans = [sum(tall for _, _, tall in blocks) for blocks, _, _ in chunks]
+    units = [max(1, wide // width) for wide in spans]
+    narrow = [wide < width for wide in spans]
     bounds = [sum(units[:n]) for n in range(len(units) + 1)]
     count = len(chunks)
 
@@ -353,6 +372,12 @@
                 hidden[src, :], w[0] if len(w) == 1 else jnp.concatenate(w, axis=0),
                 (((1,), (1,)), ((), ())), preferred_element_type=f32,
             )
+            if narrow[n]:
+                value = jnp.concatenate([
+                    jnp.concatenate([value[r:r + own_tok // 2], value[r + own_tok // 2:r + own_tok]], axis=1)
+                    for r in range(0, tile, own_tok)
+                ], axis=0)
+                at = pl.ds(pl.multiple_of(i * (tile // 2), tile // 2), tile // 2)
             for unit in range(units[n]):
                 out(unit)[at, :] = value[:, unit * width:(unit + 1) * width].astype(out(unit).dtype)
 
@@ -363,7 +388,7 @@
 
     def pair_copy(n, i=None, slot=None):
         mine = pl.ds(bounds[n], units[n])
-        at = (mine,) if slot is None else (mine, slot_rows(slot))
+        at = (mine, pl.ds(0, half // 2 if narrow[n] else half)) if slot is None else (mine, slot_rows(slot))
         return pltpu.make_async_remote_copy(
             src_ref=pair_send.at[at], dst_ref=pair_recv.at[at],
             send_sem=p_sent.at[0], recv_sem=p_got.at[n if i is None else count + i],
@@ -375,6 +400,8 @@
 
     deal = units[0]
     meets = range(first, count - 1 if n_z > 3 else first)
+    low_meets = range(first, max(first, meets.stop - 1))
+    lasting = range(max(first, count - 2), count)
 
     def chain_copy(n, side, hops):
         mine = pl.ds(n * deal, deal)
@@ -391,9 +418,11 @@
 
     def straight_copy(n, k):
         mine = pl.ds(bounds[n], units[n])
+        tall = own_tok // 2 if narrow[n] else own_tok
+        at = pl.ds(pl.multiple_of(((z + k) % n_z) * tall, tall), tall)
         return pltpu.make_async_remote_copy(
-            src_ref=z_send.at[mine, slot_rows((z + k) % n_z), :], dst_ref=z_pass.at[mine, k - 1],
-            send_sem=z_sent.at[0], recv_sem=z_got.at[n, k - 1],
+            src_ref=z_send.at[mine, at, :], dst_ref=z_pass.at[mine, k - 1, pl.ds(0, tall)],
+            send_sem=z_sent.at[0], recv_sem=f_got.at[n - first],
             device_id={"tp": z_peer(k)}, device_id_type=MESH,
         )
 
@@ -406,7 +435,7 @@
         )
 
     def meet(n):
-        for at, to in ((1, n_z - 1), (n_z - 2, 0)):
+        for at, to in ((1, n_z - 1), (n_z - 2, 0))[:2 if n in low_meets else 1]:
             @pl.when(z == at)
             def _():
                 meet_copy(n, to).wait_recv()
@@ -416,6 +445,11 @@
                     z_send[unit, rest, :] = both.astype(jnp.bfloat16)
                 straight_copy(n, (to - at) % n_z).start()
 
+    def held(n, to):
+        inner = (z > 0) & (z < n_z - 1)
+        low = (to > 0) & (to < z) if n in lasting else to < 0
+        return low | (inner & (to == z + 1)) if n == count - 1 else low
+
     def at_ends(run):
         for side, end in ((1, 0), (-1, n_z - 1)):
             @pl.when(z == end)
@@ -425,25 +459,27 @@
     def finish(n):
         pair_copy(n).wait_recv()
         for unit in range(units[n]):
-            at = bounds[n] + unit
-            z_send[at] = (pair_own[n % 2, unit] + pair_recv[at].astype(f32)).astype(jnp.bfloat16)
-        if n in meets:
+            at, rest = bounds[n] + unit, slice(0, half // 2 if narrow[n] else half)
+            z_send[at, rest, :] = (pair_own[n % 2, unit, rest, :] + pair_recv[at, rest, :].astype(f32)).astype(jnp.bfloat16)
+        if n >= first:
             for k in range(n_z - 1, 0, -1):
                 hop = jnp.where(z < n_z // 2, k, n_z - k)
                 to = (z + hop) % n_z
-                across_all = ((z == 0) & (to == n_z - 1)) | ((z == n_z - 1) & (to == 0))
-                waits = ((z == 1) & (to == n_z - 1)) | ((z == n_z - 2) & (to == 0))
-
-                @pl.when(across_all)
-                def _():
-                    meet_copy(n, to).start()
-
-                @pl.when(jnp.logical_not(across_all | waits))
+                later = held(n, to)
+                if n in meets:
+                    over, waits = (z == 0) & (to == n_z - 1), (z == 1) & (to == n_z - 1)
+                    if n in low_meets:
+                        over, waits = over | ((z == n_z - 1) & (to == 0)), waits | ((z == n_z - 2) & (to == 0))
+
+                    @pl.when(over)
+                    def _():
+                        meet_copy(n, to).start()
+
+                    later = later | over | waits
+
+                @pl.when(jnp.logical_not(later))
                 def _():
                     straight_copy(n, hop).start()
-        elif n >= first:
-            for k in range(n_z - 1, 0, -1):
-                straight_copy(n, jnp.where(z < n_z // 2, k, n_z - k)).start()
         else:
             at_ends(lambda side: [chain_copy(n, side, hops).start() for hops in range(n_z - 1, 0, -1)])
 
@@ -467,10 +503,11 @@
         for side in (1, -1):
             depth = z if side > 0 else n_z - 1 - z
             inner = (depth > 0) & (depth < n_z - 1)
-            for late in (1, 0):
-                n = t - depth - late
-                slow = (n < 2) | ((n == first - 1) & (depth > 1))
-                turn = inner & (n >= 0) & (n < first) & (slow if late else jnp.logical_not(slow))
+            for later in (1, 0):
+                n = t - depth - later
+                far = (depth > 1) * 1
+                lag = (n < 2) * 1 + (n == first - 1) * far
+                turn = inner & (n >= 0) & (n < first) & (lag == later)
 
                 @pl.when(turn)
                 def _():
@@ -545,18 +582,35 @@
         if n < first:
             with jax.named_scope(f"d{n}_relay"):
                 relay(n)
+    def free(those, which):
+        for k in range(n_z - 1, 0, -1):
+            for n in those:
+                to = (z + k) % n_z
+
+                @pl.when(held(n, to) & which(to))
+                def _():
+                    straight_copy(n, k).start()
+
+    free(lasting, lambda to: to < z)
     with jax.named_scope("lastrelay"):
-        for t in range(count, first + n_z):
+        for t in range(count, first + n_z + 2):
             relay(t)
         for n in meets:
             if n + 2 >= count:
                 meet(n)
+        free((count - 1,), lambda to: to > z)
 
     mine = slot_rows(z)
 
-    def total_of(unit):
+    def total_of(n, unit):
+        if narrow[n]:
+            short = own_tok // 2
+            branch = z_send[unit, pl.ds(pl.multiple_of(z * short, short), short), :].astype(f32)
+            for k in range(n_z - 1):
+                branch = branch + z_pass[unit, k, :short, :].astype(f32)
+            return jnp.concatenate([branch[:, :width // 2], branch[:, width // 2:]], axis=0)
         branch = z_send[unit, mine, :].astype(f32)
-        if unit < bounds[first]:
+        if n < first:
             return branch + z_last[0, unit].astype(f32) + z_last[1, unit].astype(f32)
         for k in range(n_z - 1):
             branch = branch + z_pass[unit, k].astype(f32)
@@ -582,22 +636,34 @@
     for n, (blocks, _, _) in enumerate(chunks):
         with jax.named_scope(f"last{n}"):
             if n >= first:
-                for k in range(1, n_z):
-                    absent = ((z == n_z - 1) & (k == n_z - 1)) | ((z == 0) & (k == 1))
-                    if n not in meets:
-                        straight_copy(n, k).wait_recv()
-                    elif k in (1, n_z - 1):
-                        @pl.when(jnp.logical_not(absent))
+                spread = pl.ds(bounds[n], units[n])
+                tall = own_tok // 2 if narrow[n] else own_tok
+
+                def came(many):
+                    here = z_pass.at[spread, pl.ds(0, many), pl.ds(0, tall)]
+                    pltpu.make_async_remote_copy(
+                        src_ref=here, dst_ref=here, send_sem=z_sent.at[0], recv_sem=f_got.at[n - first],
+                        device_id={"tp": sibling}, device_id_type=MESH,
+                    ).wait_recv()
+
+                if n not in meets:
+                    came(n_z - 1)
+                else:
+                    edges = ((n_z - 1, n_z - 1), (0, 1))[:2 if n in low_meets else 1]
+                    at_edge = (z == n_z - 1) | (z == 0) if n in low_meets else z == n_z - 1
+
+                    @pl.when(jnp.logical_not(at_edge))
+                    def _():
+                        came(n_z - 1)
+
+                    @pl.when(at_edge)
+                    def _():
+                        came(n_z - 2)
+                    for edge, k in edges:
+                        @pl.when(z == edge)
                         def _():
-                            straight_copy(n, k).wait_recv()
-
-                        @pl.when(absent)
-                        def _():
-                            spread = pl.ds(bounds[n], units[n])
                             z_pass[spread, k - 1] = jnp.zeros((units[n], own_tok, width), jnp.bfloat16)
-                    else:
-                        straight_copy(n, k).wait_recv()
-            sums = [total_of(unit) for unit in range(bounds[n], bounds[n + 1])]
+            sums = [total_of(n, unit) for unit in range(bounds[n], bounds[n + 1])]
             lane = 0
             for mask, top, tall in blocks:
                 if tall < width:
@@ -617,11 +683,12 @@
             device_id={"tp": sibling}, device_id_type=MESH,
         ).wait_send()
 
+    whole = pl.ds(0, n_fs * rows // width)
     for w in range(3):
         sent(ready[w].at[pl.ds(0, every * rows), :], w_sent.at[w])
     sent(tok.at[pl.ds(0, (2 * n_z - 1) * own_tok), :], t_sent.at[0])
-    sent(pair_send, p_sent.at[0])
-    sent(z_pass, z_sent.at[0])
+    sent(pair_send.at[whole], p_sent.at[0])
+    sent(z_pass.at[whole], z_sent.at[0])
 
 
 def store(*refs):
@@ -646,17 +713,18 @@
     half, total = n_z * own_tok, n_tp * own_tok
     part = rows // dims
     halves = part // 128 if part % 128 == 0 else 1
-    late_tall, tall_of, width, chunks, first = plan(n_fs, dims, rows)
-    count, deal = n_fs * rows // width, sum(tall for _, _, tall in chunks[0][0]) // width
+    late, other, width, chunks, first = plan(n_fs, dims, rows)
+    count = sum(max(1, sum(tall for _, _, tall in blocks) // width) for blocks, _, _ in chunks)
+    deal = sum(tall for _, _, tall in chunks[0][0]) // width
     steps = len(chunks)
-    pieces = dims * ((n_fs - 1) * (1 + halves) + (n_fs - 2) * (part // tall_of) + part // late_tall)
+    pieces = (1 if dims == 2 else dims) * ((n_fs - 1) * (1 + halves) + (n_fs - 2) * len(other) + len(late))
     bf16, f32 = jnp.bfloat16, jnp.float32
     dma = pltpu.SemaphoreType.DMA
     vmem = pl.BlockSpec(memory_space=pltpu.VMEM)
     hbm = pl.BlockSpec(memory_space=pltpu.HBM)
     operands = (tokens, norm_gain[None, :], gate_master, up_master, down_master)
     results = pl.pallas_call(
-        functools.partial(kernel, n_fs, n_z, dims, halves, late_tall, tall_of, width, chunks, first),
+        functools.partial(kernel, n_fs, n_z, dims, halves, late, other, width, chunks, first),
         out_shape=(pltpu.VMEM((own_tok, depth), bf16),)
         + tuple(pltpu.VMEM((n_fs * rows, cols), bf16) for _ in range(3)),
         in_specs=[hbm] * 5,
@@ -678,9 +746,9 @@
             pltpu.VMEM((count, n_z - 1, own_tok, width), bf16),
             pltpu.VMEM((2, count, own_tok, width), bf16),
             dma((3,)), dma((pieces,)),
-            dma((1,)), dma((n_z,)), dma((n_z,)),
+            dma((1,)), dma((n_z - 1,)), dma((1,)),
             dma((1,)), dma((steps + n_z,)),
-            dma((1,)), dma((steps, n_z - 1)), dma((2,)), dma((steps - first,)),
+            dma((1,)), dma((first, n_z - 1)), dma((2,)), dma((steps - first,)), dma((steps - first,)),
             dma((4 * dims + 3,)),
         ],
         compiler_params=pltpu.CompilerParams(

time: 123 us -> 122 us (level)
    pallas_call x1, Pallas kernels: 117 us -> 116 us  [body(): pl.pallas_call(functools.partial(kernel, n_fs, n_z, dims, halves, late, o...]
where the time goes in v2:
time: 122 us; the launch traced here: 121 us
  Pallas kernels  121 us (99%)
    pallas_call x1, Pallas kernels, body(): pl.pallas_call(functools.partial(kernel, n_fs, n_z, dims, halves, late, o...  116 us
    pallas_call x1, Pallas kernels, body(): pl.pallas_call(store, out_shape=tuple((jax.ShapeDtypeStruct(result.shape,...  4.84 us

profile of v2, /device:TPU:0, one launch (start us, length us, event | category | flops | bytes accessed | tf_op | source)
XLA Modules:
  0.0 121.3 jit_solution(2647451139675704996)
XLA Ops:
  0.6 115.9 %shard_map.84 = (bf16[128,2048]{1,0:T(8,128)(2,1)S(1)}, bf16[2048,1024]{1,0:T(8,128)(2,1)S(1)}, bf16[2048,1024]{1,0:T(8,128)(2,1)S(1)}, bf16[2048,1024]{1,0:T(8,128)(2,1)S(1)}) custom-call(bf16[128,2048]{1,0:T(8,128)(2,1)} %tok_hbm.1, f32[1,512]{1,0:T(1,128)} %bitcast.1, f32[512,1024]{1,0:T(8,128)} %gate_hbm.1, f32[512,1024]{1,0:T(8,128)} %up_hbm.1, ...), custom_call_target="tpu_custom_call" | custom-call | tf_op jit(solution)/shard_map/pallas_call | solution.py:726
  116.5 4.8 %shard_map.85 = (bf16[128,2048]{1,0:T(8,128)(2,1)}, bf16[2048,1024]{1,0:T(8,128)(2,1)}, bf16[2048,1024]{1,0:T(8,128)(2,1)}, bf16[2048,1024]{1,0:T(8,128)(2,1)}) custom-call(bf16[128,2048]{1,0:T(8,128)(2,1)S(1)} %get-tuple-element.8.refs_0_, bf16[2048,1024]{1,0:T(8,128)(2,1)S(1)} %get-tuple-element.9.refs_1_, ...), custom_call_target="tpu_custom_call" | custom-call | tf_op jit(solution)/shard_map/pallas_call | solution.py:758

commit v3 on v2

--- a/solution.py
+++ b/solution.py
@@ -553,8 +553,6 @@
     for n, (blocks, needs, wave) in enumerate(chunks):
         if n == 0:
             continue
-        if split and n == 3:
-            send_down(0, range(1, dims))
         for p, h, mask in needs:
             with jax.named_scope(f"d{n}_need"):
                 need(DOWN, p, h, mask, hold=split and n in (2, 3))
@@ -575,6 +573,8 @@
                 finished = n
         with jax.named_scope(f"d{n}_prodB"):
             product(n, core, lambda unit: pair_own.at[n % 2, unit])
+        if split and n == 2:
+            send_down(0, range(1, dims))
         if n + 1 == count or chunks[n + 1][2] != wave:
             with jax.named_scope(f"d{n}_finish"):
                 finish(n)

time: 122 us -> 121 us (level)
  no operation moved by 1% of the time
where the time goes in v3:
time: 121 us
  Pallas kernels  121 us (100%)
    pallas_call x1, Pallas kernels, body(): pl.pallas_call(functools.partial(kernel, n_fs, n_z, dims, halves, late, o...  116 us
    pallas_call x1, Pallas kernels, body(): pl.pallas_call(store, out_shape=tuple((jax.ShapeDtypeStruct(result.shape,...  4.84 us

profile of v3, /device:TPU:0, one launch (start us, length us, event | category | flops | bytes accessed | tf_op | source)
XLA Modules:
  0.0 121.3 jit_solution(3015036859110662735)
XLA Ops:
  0.6 115.8 %shard_map.84 = (bf16[128,2048]{1,0:T(8,128)(2,1)S(1)}, bf16[2048,1024]{1,0:T(8,128)(2,1)S(1)}, bf16[2048,1024]{1,0:T(8,128)(2,1)S(1)}, bf16[2048,1024]{1,0:T(8,128)(2,1)S(1)}) custom-call(bf16[128,2048]{1,0:T(8,128)(2,1)} %tok_hbm.1, f32[1,512]{1,0:T(1,128)} %bitcast.1, f32[512,1024]{1,0:T(8,128)} %gate_hbm.1, f32[512,1024]{1,0:T(8,128)} %up_hbm.1, ...), custom_call_target="tpu_custom_call" | custom-call | tf_op jit(solution)/shard_map/pallas_call | solution.py:726
  116.5 4.8 %shard_map.85 = (bf16[128,2048]{1,0:T(8,128)(2,1)}, bf16[2048,1024]{1,0:T(8,128)(2,1)}, bf16[2048,1024]{1,0:T(8,128)(2,1)}, bf16[2048,1024]{1,0:T(8,128)(2,1)}) custom-call(bf16[128,2048]{1,0:T(8,128)(2,1)S(1)} %get-tuple-element.8.refs_0_, bf16[2048,1024]{1,0:T(8,128)(2,1)S(1)} %get-tuple-element.9.refs_1_, ...), custom_call_target="tpu_custom_call" | custom-call | tf_op jit(solution)/shard_map/pallas_call | solution.py:758
